TPU v7x, 32 devices: a whole 2x2x4 slice. The times are simulated.
32 devices in a mesh: sp: 16 (over z, y, x), tp: 2 (over core).
Axes of the slice: x: 2, y: 2, z: 4, core: 2. Of those that a mesh axis runs over, the one named last changes fastest.
Arguments:
- residual: bfloat16 [2048, 2048], P('sp'), may hold values from -6 to 6
- query_first: bfloat16 [2048, 8, 128], P('sp', 'tp'), may hold values from -6.5 to 6.5
- key_first: bfloat16 [2048, 8, 128], P('sp', 'tp'), may hold values from -6.5 to 6.5
- value_first: bfloat16 [2048, 8, 128], P('sp', 'tp'), may hold values from -6 to 6
- query_second: bfloat16 [2048, 8, 64], P('sp', 'tp'), may hold values from -6.5 to 6.5
- key_second: bfloat16 [2048, 8, 64], P('sp', 'tp'), may hold values from -6.5 to 6.5
- value_second: bfloat16 [2048, 8, 64], P('sp', 'tp'), may hold values from -6 to 6
- balance_first: float32 [8], P('tp'), may hold values from 0.3 to 0.8
- balance_second: float32 [8], P('tp'), may hold values from 0.3 to 0.8
- head_gain_first: float32 [128], replicated, may hold values from 0.1 to 1.9
- head_gain_second: float32 [64], replicated, may hold values from 0.1 to 1.9
- out_first: bfloat16 [1024, 2048], P('tp'), may hold values from -0.15625 to 0.15625
- out_second: bfloat16 [512, 2048], P('tp'), may hold values from -0.15625 to 0.15625
- mlp_gain: float32 [2048], replicated, may hold values from 0.1 to 1.9
- up_weight: bfloat16 [2048, 8192], P('sp', 'tp'), may hold values from -0.125 to 0.125
- down_weight: bfloat16 [2048, 8192], P('sp', 'tp'), may hold values from -0.0625 to 0.0625
Outputs:
- layer_out: bfloat16 [2048, 2048], P('sp')
All inputs are finite; a program needn't handle non-finite values.
Results may differ from a plain program's by a relative error of at most 0.018.
Values may be sent and summed in bfloat16 or wider, within the bound.
A program may use at most 128 MiB of HBM per device.

v0:
```python
import math

import jax
import jax.numpy as jnp
from jax import lax
from jax.sharding import PartitionSpec as P

DK_A = 64
DK_B = 32


EPSILON = 1e-06
HEAD_SCALE = 0.8


def attend(queries, keys, values, balance, gain, device, head_size):
    tokens = queries.shape[0]
    heads = queries.shape[1]
    seq = keys.shape[0]
    depth = values.shape[2]
    block = math.gcd(512, seq)
    scale = head_size ** (-0.5)
    query_maps = queries.reshape(tokens, heads, 2, head_size)
    key_maps = keys.reshape(seq, heads, 2, head_size)
    first_row = device * tokens
    positions = first_row + jnp.arange(tokens, dtype=jnp.int32)
    needed = (first_row + tokens + block - 1) // block

    def block_scores(number):
        start = number * block
        key_block = lax.dynamic_slice_in_dim(key_maps, start, block, 0)
        scores = (
            jnp.einsum("qhmd,khmd->hmqk", query_maps, key_block, preferred_element_type=jnp.float32)
            * scale
        )
        columns = start + jnp.arange(block, dtype=jnp.int32)
        visible = columns[None, :] <= positions[:, None]
        return (jnp.where(visible, scores, -jnp.inf), start)

    def statistics(number, carry):
        highest, total = carry
        scores, start = block_scores(number)
        fresh = jnp.maximum(highest, jnp.max(scores, axis=-1, keepdims=True))
        total = total * jnp.exp(highest - fresh) + jnp.sum(
            jnp.exp(scores - fresh), axis=-1, keepdims=True
        )
        return (fresh, total)

    start_high = jnp.full((heads, 2, tokens, 1), -jnp.inf, jnp.float32)
    start_total = jnp.zeros((heads, 2, tokens, 1), jnp.float32)
    highest, total = lax.fori_loop(0, needed, statistics, (start_high, start_total))

    def accumulate(number, result):
        scores, start = block_scores(number)
        probs = jnp.exp(scores - highest) / total
        mixed = (probs[:, 0] - balance[:, None, None] * probs[:, 1]).astype(jnp.bfloat16)
        value_block = lax.dynamic_slice_in_dim(values, start, block, 0)
        return result + jnp.einsum(
            "hqk,khe->qhe", mixed, value_block, preferred_element_type=jnp.float32
        )

    summed = lax.fori_loop(0, needed, accumulate, jnp.zeros((tokens, heads, depth), jnp.float32))
    power = jnp.mean(summed * summed, axis=-1, keepdims=True)
    normed = summed * lax.rsqrt(power + EPSILON) * gain * HEAD_SCALE
    return normed.astype(jnp.bfloat16).reshape(tokens, heads * depth)


def body(
    residual,
    query_first,
    key_first,
    value_first,
    query_second,
    key_second,
    value_second,
    balance_first,
    balance_second,
    head_gain_first,
    head_gain_second,
    out_first,
    out_second,
    mlp_gain,
    up_weight,
    down_weight,
):
    device = lax.axis_index("sp")
    keys_first, values_first, keys_second, values_second = (
        lax.all_gather(key_first, "sp", axis=0, tiled=True),
        lax.all_gather(value_first, "sp", axis=0, tiled=True),
        lax.all_gather(key_second, "sp", axis=0, tiled=True),
        lax.all_gather(value_second, "sp", axis=0, tiled=True),
    )
    heads_first = attend(
        query_first, keys_first, values_first, balance_first, head_gain_first, device, DK_A
    )
    heads_second = attend(
        query_second, keys_second, values_second, balance_second, head_gain_second, device, DK_B
    )
    head_term = jnp.dot(heads_first, out_first, preferred_element_type=jnp.float32) + jnp.dot(
        heads_second, out_second, preferred_element_type=jnp.float32
    )
    head_total = lax.psum(head_term.astype(jnp.bfloat16), "tp").astype(jnp.float32)
    mixed = (residual.astype(jnp.float32) + head_total).astype(jnp.bfloat16)
    mixed_float = mixed.astype(jnp.float32)
    power = jnp.mean(mixed_float * mixed_float, axis=-1, keepdims=True)
    normed = (mixed_float * lax.rsqrt(power + EPSILON) * mlp_gain).astype(jnp.bfloat16)
    up_whole, down_whole = (
        lax.all_gather(up_weight, "sp", axis=0, tiled=True),
        lax.all_gather(down_weight, "sp", axis=0, tiled=True),
    )
    lifted = jnp.dot(normed, up_whole, preferred_element_type=jnp.float32)
    active = jax.nn.relu(lifted)
    hidden = (active * active).astype(jnp.bfloat16)
    down_term = lax.dot_general(
        hidden, down_whole, (((1,), (1,)), ((), ())), preferred_element_type=jnp.float32
    )
    added = lax.psum(down_term.astype(jnp.bfloat16), "tp").astype(jnp.float32)
    return (mixed_float + added).astype(jnp.bfloat16)


def solution(mesh):
    in_specs = (
        P("sp", None),
        P("sp", "tp", None),
        P("sp", "tp", None),
        P("sp", "tp", None),
        P("sp", "tp", None),
        P("sp", "tp", None),
        P("sp", "tp", None),
        P("tp"),
        P("tp"),
        P(),
        P(),
        P("tp", None),
        P("tp", None),
        P(),
        P("sp", "tp"),
        P("sp", "tp"),
    )
    out_specs = P("sp", None)
    return jax.shard_map(body, mesh=mesh, in_specs=in_specs, out_specs=out_specs, check_vma=False)
```

profile of v0, /device:TPU:0, one launch (start us, length us, event | category | flops | bytes accessed | tf_op | source)
XLA Modules:
  0.0 704.4 jit_solution(6318953147037284549)
XLA Ops:
  6.5 0.7 all-gather.13.cloned.1.call-update
  7.3 0.7 all-gather.11.cloned.1.call-update
  8.1 0.7 all-gather.9.cloned.1.call-update
  8.8 1.7 copy.36
  10.5 1.0 copy.38
  11.6 52.6 %all-gather.13.cloned.1.call-done = bf16[2048,4,64]{0,2,1:T(8,128)(2,1)} async-done(((bf16[128,4,64]{0,2,1:T(8,128)(2,1)}), bf16[2048,4,64]{0,2,1:T(8,128)(2,1)}) %all-gather.13.cloned.1.call-update) | async-done | bytes 1048592 | tf_op jit(solution)/shard_map/all_gather | solution.py:90
  64.2 2.2 while.50
  64.3 1.5 fusion.92
  65.9 0.4 exponential_reduce_fusion.5
  66.4 50.9 %all-gather.11.cloned.1.call-done = bf16[2048,4,64]{0,2,1:T(8,128)(2,1)} async-done(((bf16[128,4,64]{0,2,1:T(8,128)(2,1)}), bf16[2048,4,64]{0,2,1:T(8,128)(2,1)}) %all-gather.11.cloned.1.call-update) | async-done | bytes 1048592 | tf_op jit(solution)/shard_map/all_gather | solution.py:91
  117.3 3.2 while.51
  117.5 1.7 fusion.97
  119.2 1.3 fusion.98
  120.7 1.6 fusion.56
  122.2 57.3 %all-gather.9.cloned.1.call-done = bf16[2048,4,128]{2,1,0:T(4,128)(2,1)} async-done(((bf16[128,4,128]{2,1,0:T(4,128)(2,1)}), bf16[2048,4,128]{2,1,0:T(4,128)(2,1)}) %all-gather.9.cloned.1.call-update) | async-done | bytes 2097168 | tf_op jit(solution)/shard_map/all_gather | solution.py:88
  179.5 4.3 copy.37
  183.9 2.3 while.48
  184.1 1.6 fusion.84
  186.2 57.7 %all-gather.7.cloned.1.call-done = bf16[2048,4,128]{0,2,1:T(8,128)(2,1)} async-done(((bf16[128,4,128]{0,2,1:T(8,128)(2,1)}), bf16[2048,4,128]{0,2,1:T(8,128)(2,1)}) %all-gather.7.cloned.1.call-update) | async-done | bytes 2097168 | tf_op jit(solution)/shard_map/all_gather | solution.py:89
  243.9 3.4 while.49
  244.1 1.8 fusion.89
  245.9 1.4 fusion.90
  247.5 1.3 fusion.44
  248.8 0.5 all-gather.15.cloned.1.call-update
  249.4 0.7 all-gather.17.cloned.1.call-update
  250.2 25.8 %all-reduce.3.cloned.1.call-done = bf16[128,2048]{1,0:T(8,128)(2,1)} async-done(((bf16[128,2048]{1,0:T(8,128)(2,1)}), bf16[128,2048]{1,0:T(8,128)(2,1)}) %all-reduce.3.cloned.1.call-update) | async-done | bytes 524304 | tf_op jit(solution)/shard_map/psum | solution.py:102
  275.9 1.3 fusion.45
  277.2 193.6 %all-gather.15.cloned.1.call-done = bf16[2048,4096]{1,0:T(8,128)(2,1)} async-done(((bf16[128,4096]{1,0:T(8,128)(2,1)}), bf16[2048,4096]{1,0:T(8,128)(2,1)}) %all-gather.15.cloned.1.call-update) | async-done | bytes 16777232 | tf_op jit(solution)/shard_map/all_gather | solution.py:108
  470.8 192.0 %all-gather.17.cloned.1.call-done = bf16[2048,4096]{1,0:T(8,128)(2,1)} async-done(((bf16[128,4096]{1,0:T(8,128)(2,1)}), bf16[2048,4096]{1,0:T(8,128)(2,1)}) %all-gather.17.cloned.1.call-update) | async-done | bytes 16777232 | tf_op jit(solution)/shard_map/all_gather | solution.py:109
  662.8 15.7 %convolution_convert_fusion = bf16[128,2048]{1,0:T(8,128)(2,1)} fusion(bf16[2048,4096]{1,0:T(8,128)(2,1)} %all-gather.17.cloned.1.call-done, bf16[2048,4096]{1,0:T(8,128)(2,1)} %all-gather.15.cloned.1.call-done, f32[2048]{0:T(1024)S(1)} %copy-done.5, f32[128]{0:T(128)S(1)} %add_rsqrt_fusion.2, bf16[128,2048]{1,0:T(8,128)(2,1)} %all-reduce.3.cloned.1.call-done, ...), kind=kOutput, calls=%fused_computation.69 | convolution fusion | flops 4298899456 | bytes 35136000 | tf_op jit(solution)/shard_map/dot_general | solution.py:114
  678.5 16.9 %all-reduce.5.cloned.1.call-done = bf16[128,2048]{1,0:T(8,128)(2,1)} async-done(((bf16[128,2048]{1,0:T(8,128)(2,1)}), bf16[128,2048]{1,0:T(8,128)(2,1)}) %all-reduce.5.cloned.1.call-update) | async-done | bytes 524304 | tf_op jit(solution)/shard_map/psum | solution.py:117
  695.5 2.1 fusion.48
  (59 shorter events, 1.7 us)
Async XLA Ops:
  6.5 241.0 %copy-start = (bf16[512,2048]{1,0:T(8,128)(2,1)S(1)}, bf16[512,2048]{1,0:T(8,128)(2,1)}, u32[]{:S(2)}) copy-start(bf16[512,2048]{1,0:T(8,128)(2,1)} %param.35) | copy-start | bytes 6291460
  6.5 57.6 %all-gather.13.cloned.1.call-start = ((), (), s32[]{:S(2)}) async-start(), calls=%async_computation.3 | async-start | bytes 1114112 | tf_op jit(solution)/shard_map/all_gather | solution.py:90
  7.3 110.1 %all-gather.11.cloned.1.call-start = ((), (), s32[]{:S(2)}) async-start(), calls=%async_computation.2 | async-start | bytes 1114112 | tf_op jit(solution)/shard_map/all_gather | solution.py:91
  8.0 171.5 %all-gather.9.cloned.1.call-start = ((), (), s32[]{:S(2)}) async-start(), calls=%async_computation.1 | async-start | bytes 2228224 | tf_op jit(solution)/shard_map/all_gather | solution.py:88
  8.7 235.1 %all-gather.7.cloned.1.call-start = ((), (), s32[]{:S(2)}) async-start(), calls=%async_computation | async-start | bytes 2228224 | tf_op jit(solution)/shard_map/all_gather | solution.py:89
  10.5 265.4 %all-reduce.3.cloned.1.call-start = ((), (), s32[]{:S(2)}) async-start(), calls=%async_computation.4 | async-start | bytes 1048576 | tf_op jit(solution)/shard_map/psum | solution.py:102
  64.2 53.1 %copy-start.3 = (f32[4]{0:T(128)S(1)}, f32[4]{0:T(128)}, u32[]{:S(2)}) copy-start(f32[4]{0:T(128)} %param.32) | copy-start | bytes 52
  117.3 3.2 copy-start.6
  183.9 60.0 %copy-start.4 = (f32[4]{0:T(128)S(1)}, f32[4]{0:T(128)}, u32[]{:S(2)}) copy-start(f32[4]{0:T(128)} %param.31) | copy-start | bytes 52
  243.9 3.5 copy-start.7
  248.8 27.2 %copy-start.1 = (bf16[128,2048]{1,0:T(8,128)(2,1)S(1)}, bf16[128,2048]{1,0:T(8,128)(2,1)}, u32[]{:S(2)}) copy-start(bf16[128,2048]{1,0:T(8,128)(2,1)} %param.24) | copy-start | bytes 1572868
  248.8 414.0 %copy-start.5 = (f32[2048]{0:T(1024)S(1)}, f32[2048]{0:T(1024)}, u32[]{:S(2)}) copy-start(f32[2048]{0:T(1024)} %param.37) | copy-start | bytes 24580
  248.8 222.0 %all-gather.15.cloned.1.call-start = ((), (), s32[]{:S(2)}) async-start(), calls=%async_computation.5 | async-start | bytes 17825792 | tf_op jit(solution)/shard_map/all_gather | solution.py:108
  249.4 413.4 %all-gather.17.cloned.1.call-start = ((), (), s32[]{:S(2)}) async-start(), calls=%async_computation.6 | async-start | bytes 17825792 | tf_op jit(solution)/shard_map/all_gather | solution.py:109
  250.1 445.3 %all-reduce.5.cloned.1.call-start = ((), (), s32[]{:S(2)}) async-start(), calls=%async_computation.7 | async-start | bytes 1048576 | tf_op jit(solution)/shard_map/psum | solution.py:117
  277.2 418.2 %copy-start.2 = (bf16[128,2048]{1,0:T(8,128)(2,1)S(1)}, bf16[128,2048]{1,0:T(8,128)(2,1)}, u32[]{:S(2)}) copy-start(bf16[128,2048]{1,0:T(8,128)(2,1)} %all-reduce.3.cloned.1.call-done) | copy-start | bytes 1572868
Sparse Core Ops, SparseCore 0:
  10.0 54.0 all-gather.12
  66.9 50.3 all-gather.10
  120.1 59.3 all-gather.8
  182.1 61.7 all-gather.6
  248.9 26.9 all-reduce.2
  278.5 192.1 all-gather.14
  473.6 189.1 all-gather.16
  678.6 16.7 all-reduce.4
where the time goes:
time: 705 us; the launch traced here: 704 us
  waiting for transfers between devices  650 us (92%)
  matrix products  27.9 us (4%)
  between operations  13.7 us (2%)
  local copies, waits for them, and re-layouts  7.12 us (1%)
    all_gather x1, waiting for transfers between devices, body(): lax.all_gather(up_weight, 'sp', axis=0, tiled=True)  194 us
    all_gather x1, waiting for transfers between devices, body(): lax.all_gather(down_weight, 'sp', axis=0, tiled=True)  192 us
    all_gather x1, waiting for transfers between devices, body(): lax.all_gather(value_first, 'sp', axis=0, tiled=True)  57.7 us
    all_gather x1, waiting for transfers between devices, body(): lax.all_gather(key_first, 'sp', axis=0, tiled=True)  57.3 us
    all_gather x1, waiting for transfers between devices, body(): lax.all_gather(key_second, 'sp', axis=0, tiled=True)  52.6 us
    all_gather x1, waiting for transfers between devices, body(): lax.all_gather(value_second, 'sp', axis=0, tiled=True)  50.9 us
    psum x1, waiting for transfers between devices, body(): lax.psum(head_term.astype(jnp.bfloat16), 'tp').astype(jnp.float32)  25.8 us
    psum x1, waiting for transfers between devices, body(): added = lax.psum(down_term.astype(jnp.bfloat16), 'tp').astype(jnp.float32)  16.9 us
  transfers between devices with their start and end apart: 8, of which 8 were waited for; matrix products, arithmetic and copies ran while one was open for 2% of the time, Pallas kernels for 0%

commit v1 on v0

--- a/solution.py
+++ b/solution.py
@@ -1,8 +1,11 @@
+import functools
 import math
 
 import jax
 import jax.numpy as jnp
 from jax import lax
+from jax.experimental import pallas as pl
+from jax.experimental.pallas import tpu as pltpu
 from jax.sharding import PartitionSpec as P
 
 DK_A = 64
@@ -118,6 +121,468 @@
     return (mixed_float + added).astype(jnp.bfloat16)
 
 
+PLANE = 4
+MESH = pl.DeviceIdType.MESH
+VMEM_BYTES = 60 * 1024 * 1024
+
+
+def remote(src, dst, send_sem, recv_sem, device):
+    return pltpu.make_async_remote_copy(
+        src_ref=src, dst_ref=dst, send_sem=send_sem, recv_sem=recv_sem,
+        device_id=device, device_id_type=MESH,
+    )
+
+
+def meet(devices):
+    barrier = pltpu.get_barrier_semaphore()
+    for device in devices:
+        pl.semaphore_signal(barrier, inc=1, device_id=device, device_id_type=MESH)
+    pl.semaphore_wait(barrier, len(devices))
+
+
+def places():
+    s = lax.axis_index("sp")
+    c = lax.axis_index("tp")
+    z = s // PLANE
+    p = s % PLANE
+    x = p % 2
+    y = p // 2
+    flip_x = y * 2 + 1 - x
+    flip_y = (1 - y) * 2 + x
+    near = (1 - c) * flip_x + c * flip_y
+    side = (1 - c) * flip_y + c * flip_x
+    far = (1 - y) * 2 + 1 - x
+    return s, c, z, p, near, side, far
+
+
+def exchange_kernel(
+    line, kv, q, up, down, kv_all, q_all, up_all, down_all,
+    local, zs, zr, qs, qr, ps, pr, us, ur, ds, dr,
+):
+    s, c, z, p, near, side, far = places()
+    n = line * PLANE
+    width = up_all.shape[2]
+    meet([((s + k) % n, c) for k in range(1, n)])
+    own = pl.ds(pl.multiple_of(s * width, width), width)
+    locals_ = [
+        pltpu.make_async_copy(kv.at[z], kv_all.at[s], local.at[0]),
+        pltpu.make_async_copy(q.at[z], q_all.at[z], local.at[1]),
+        pltpu.make_async_copy(up.at[:, own], up_all.at[s], local.at[2]),
+        pltpu.make_async_copy(down.at[:, own], down_all.at[s], local.at[3]),
+    ]
+    for copy in locals_:
+        copy.start()
+    sends = []
+
+    def send(*args):
+        copy = remote(*args)
+        copy.start()
+        sends.append(copy)
+
+    for j in range(1, line):
+        zt = (z + j) % line
+        to = (zt * PLANE + p, c)
+        send(kv.at[zt], kv_all.at[s], zs.at[j], zr.at[j], to)
+        send(q.at[zt], q_all.at[z], qs.at[j], qr.at[j], to)
+
+    def weights(ks):
+        for k in ks:
+            t = (s + k) % n
+            columns = pl.ds(pl.multiple_of(t * width, width), width)
+            send(up.at[:, columns], up_all.at[s], us.at[k], ur.at[k], (t, c))
+            send(down.at[:, columns], down_all.at[s], ds.at[k], dr.at[k], (t, c))
+
+    ring = list(range(1, n))
+    share = -(-len(ring) // line)
+    locals_[0].wait()
+    to_near = (z * PLANE + near, c)
+    to_side = (z * PLANE + side, c)
+    for j in range(line):
+        zf = (z + line - j) % line
+        block = kv_all.at[zf * PLANE + p]
+        if j:
+            remote(block, block, zs.at[j], zr.at[j], to_near).wait_recv()
+        send(block, block, ps.at[j, 0], pr.at[j, 0], to_near)
+        send(block, block, ps.at[j, 1], pr.at[j, 1], to_side)
+        weights(ring[j * share:(j + 1) * share])
+    for j in range(line):
+        zf = (z + line - j) % line
+        block = kv_all.at[zf * PLANE + near]
+        remote(block, block, ps.at[j, 0], pr.at[j, 0], to_near).wait_recv()
+        send(block, block, ps.at[j, 2], pr.at[j, 2], to_side)
+    for j in range(line):
+        zf = (z + line - j) % line
+        for way, place in ((1, side), (2, far)):
+            block = kv_all.at[zf * PLANE + place]
+            remote(block, block, ps.at[j, way], pr.at[j, way], to_side).wait_recv()
+    for j in range(1, line):
+        zf = (z + line - j) % line
+        block = q_all.at[zf]
+        remote(block, block, qs.at[j], qr.at[j], to_near).wait_recv()
+    for k in range(1, n):
+        f = (s + n - k) % n
+        remote(up_all.at[f], up_all.at[f], us.at[k], ur.at[k], to_near).wait_recv()
+        remote(down_all.at[f], down_all.at[f], ds.at[k], dr.at[k], to_near).wait_recv()
+    for copy in locals_[1:]:
+        copy.wait()
+    for copy in sends:
+        copy.wait_send()
+
+
+def exchange(line, kv, q, up, down):
+    n = line * PLANE
+    width = up.shape[1] // n
+    dma = pltpu.SemaphoreType.DMA
+    vmem = pl.BlockSpec(memory_space=pltpu.VMEM)
+    return pl.pallas_call(
+        functools.partial(exchange_kernel, line),
+        out_shape=(
+            jax.ShapeDtypeStruct((n,) + kv.shape[1:], kv.dtype),
+            jax.ShapeDtypeStruct(q.shape, q.dtype),
+            jax.ShapeDtypeStruct((n, up.shape[0], width), up.dtype),
+            jax.ShapeDtypeStruct((n, down.shape[0], width), down.dtype),
+        ),
+        in_specs=[vmem] * 4,
+        out_specs=(vmem,) * 4,
+        scratch_shapes=[
+            dma((4,)), dma((line,)), dma((line,)), dma((line,)), dma((line,)),
+            dma((line, 3)), dma((line, 3)), dma((n,)), dma((n,)), dma((n,)), dma((n,)),
+        ],
+        compiler_params=pltpu.CompilerParams(
+            collective_id=0, has_side_effects=True, vmem_limit_bytes=32 * 1024 * 1024
+        ),
+    )(kv, q, up, down)
+
+
+def last(a, b):
+    return lax.dot_general(a, b, (((1,), (1,)), ((), ())), preferred_element_type=jnp.float32)
+
+
+def attention_kernel(line, size_a, size_b, balance, q, kv, gain_a, gain_b, out):
+    s, c, z, p, _, _, _ = places()
+    tokens = q.shape[1]
+    wide = gain_a.shape[1]
+    deep = gain_b.shape[1]
+    span = PLANE * tokens
+    lanes = lax.broadcasted_iota(jnp.int32, (tokens, wide), 1)
+    rows = lax.broadcasted_iota(jnp.int32, (tokens, span), 0) + p * tokens
+    visible = lax.broadcasted_iota(jnp.int32, (tokens, span), 1) <= rows
+
+    def mix(queries, keys_at, values_at, size, b, keys_number):
+        maps = []
+        for m in range(2):
+            chosen = (lanes >= m * size) & (lanes < (m + 1) * size)
+            picked = jnp.where(chosen, queries, jnp.zeros_like(queries))
+            scores = last(picked, kv[0:keys_number, keys_at]) * size ** (-0.5)
+            tail_scores = jnp.where(visible, scores[:, keys_number - span:], -jnp.inf)
+            if keys_number > span:
+                scores = jnp.concatenate([scores[:, : keys_number - span], tail_scores], axis=1)
+            else:
+                scores = tail_scores
+            powers = jnp.exp(scores - jnp.max(scores, axis=-1, keepdims=True))
+            maps.append((powers, jnp.sum(powers, axis=-1, keepdims=True)))
+        (e1, l1), (e2, l2) = maps
+        weights = (e1 * (1.0 / l1) - e2 * (b / l2)).astype(jnp.bfloat16)
+        return jnp.dot(weights, kv[0:keys_number, values_at], preferred_element_type=jnp.float32)
+
+    def norm(mixed, gain):
+        power = jnp.mean(mixed * mixed, axis=-1, keepdims=True)
+        return (mixed * lax.rsqrt(power + EPSILON) * gain[...] * HEAD_SCALE).astype(jnp.bfloat16)
+
+    for j in range(line):
+        number = (j + 1) * span
+        first = mix(q[j, :, 0:wide], slice(0, wide), slice(wide, 2 * wide), size_a, balance[0], number)
+        out[j, :, 0:wide] = norm(first, gain_a)
+        both = slice(2 * wide, 3 * wide)
+        second = mix(q[j, :, wide:2 * wide], both, both, size_b, balance[1], number)
+        out[j, :, wide:wide + deep] = norm(second[:, wide - deep:wide], gain_b)
+
+
+def attention(line, size_a, size_b, balance, q, kv, gain_a, gain_b):
+    vmem = pl.BlockSpec(memory_space=pltpu.VMEM)
+    shape = (line, q.shape[1], gain_a.shape[1] + gain_b.shape[1])
+    return pl.pallas_call(
+        functools.partial(attention_kernel, line, size_a, size_b),
+        out_shape=jax.ShapeDtypeStruct(shape, jnp.bfloat16),
+        in_specs=[pl.BlockSpec(memory_space=pltpu.SMEM)] + [vmem] * 4,
+        out_specs=vmem,
+        compiler_params=pltpu.CompilerParams(vmem_limit_bytes=32 * 1024 * 1024),
+    )(balance, q, kv, gain_a, gain_b)
+
+
+def return_kernel(line, heads, gathered, local, zs, zr):
+    s, c, z, p, _, _, _ = places()
+    meet([(((z + j) % line) * PLANE + p, c) for j in range(1, line)])
+    mine = pltpu.make_async_copy(heads.at[z], gathered.at[z], local)
+    mine.start()
+    sends = []
+    for j in range(1, line):
+        zt = (z + j) % line
+        copy = remote(heads.at[zt], gathered.at[z], zs.at[j], zr.at[j], (zt * PLANE + p, c))
+        copy.start()
+        sends.append(copy)
+    for j in range(1, line):
+        block = gathered.at[(z + line - j) % line]
+        remote(block, block, zs.at[j], zr.at[j], (s, 1 - c)).wait_recv()
+    mine.wait()
+    for copy in sends:
+        copy.wait_send()
+
+
+def return_heads(line, heads):
+    dma = pltpu.SemaphoreType.DMA
+    vmem = pl.BlockSpec(memory_space=pltpu.VMEM)
+    return pl.pallas_call(
+        functools.partial(return_kernel, line),
+        out_shape=jax.ShapeDtypeStruct(heads.shape, heads.dtype),
+        in_specs=[vmem],
+        out_specs=vmem,
+        scratch_shapes=[dma, dma((line,)), dma((line,))],
+        compiler_params=pltpu.CompilerParams(collective_id=1, has_side_effects=True),
+    )(heads)
+
+
+def gather_kernel(
+    line, residual, part, gain, mixed, rows, other_part, xs, xr, zs, zr, ps, pr, cs, cr
+):
+    s, c, z, p, near, side, far = places()
+    to_near = (z * PLANE + near, c)
+    to_side = (z * PLANE + side, c)
+    to_core = (s, 1 - c)
+    meet(
+        [to_near, to_side, to_core]
+        + [(((z + j) % line) * PLANE + p, c) for j in range(1, line)]
+    )
+    swap = remote(part.at[1 - c], other_part, xs, xr, to_core)
+    swap.start()
+    swap.wait()
+    total = part[c].astype(jnp.float32) + other_part[...].astype(jnp.float32)
+    mixed[...] = (residual[c].astype(jnp.float32) + total).astype(jnp.bfloat16)
+    whole = mixed[...].astype(jnp.float32)
+    power = jnp.mean(whole * whole, axis=-1, keepdims=True)
+    rows[s * 2 + c] = (whole * lax.rsqrt(power + EPSILON) * gain[...]).astype(jnp.bfloat16)
+    sends = []
+
+    def send(block, send_sem, recv_sem, device):
+        copy = remote(block, block, send_sem, recv_sem, device)
+        copy.start()
+        sends.append(copy)
+
+    def arrived(block, send_sem, recv_sem):
+        remote(block, block, send_sem, recv_sem, to_core).wait_recv()
+
+    def slot(j, place, core):
+        return rows.at[(((z + line - j) % line) * PLANE + place) * 2 + core]
+
+    for j in range(1, line):
+        send(slot(0, p, c), zs.at[j], zr.at[j], (((z + j) % line) * PLANE + p, c))
+    for j in range(line + 1):
+        if j < line:
+            block = slot(j, p, c)
+            if j:
+                arrived(block, zs.at[j], zr.at[j])
+            send(block, ps.at[j, 0], pr.at[j, 0], to_near)
+            send(block, ps.at[j, 1], pr.at[j, 1], to_side)
+            send(block, cs.at[j, 0], cr.at[j, 0], to_core)
+        if j:
+            block = slot(j - 1, near, c)
+            arrived(block, ps.at[j - 1, 0], pr.at[j - 1, 0])
+            send(block, ps.at[j - 1, 2], pr.at[j - 1, 2], to_side)
+            send(block, cs.at[j - 1, 1], cr.at[j - 1, 1], to_core)
+    for j in range(line):
+        for way, place in ((1, side), (2, far)):
+            block = slot(j, place, c)
+            arrived(block, ps.at[j, way], pr.at[j, way])
+            send(block, cs.at[j, 1 + way], cr.at[j, 1 + way], to_core)
+    for j in range(line):
+        for way, place in enumerate((p, side, near, far)):
+            arrived(slot(j, place, 1 - c), cs.at[j, way], cr.at[j, way])
+    for copy in sends:
+        copy.wait_send()
+
+
+def gather_rows(line, residual, part, gain):
+    dma = pltpu.SemaphoreType.DMA
+    vmem = pl.BlockSpec(memory_space=pltpu.VMEM)
+    _, half, features = part.shape
+    return pl.pallas_call(
+        functools.partial(gather_kernel, line),
+        out_shape=(
+            jax.ShapeDtypeStruct((half, features), jnp.bfloat16),
+            jax.ShapeDtypeStruct((line * PLANE * 2, half, features), jnp.bfloat16),
+        ),
+        in_specs=[vmem] * 3,
+        out_specs=(vmem, vmem),
+        scratch_shapes=[
+            pltpu.VMEM((half, features), jnp.bfloat16), dma, dma,
+            dma((line,)), dma((line,)), dma((line, 3)), dma((line, 3)), dma((line, 4)), dma((line, 4)),
+        ],
+        compiler_params=pltpu.CompilerParams(
+            collective_id=2, has_side_effects=True, vmem_limit_bytes=24 * 1024 * 1024
+        ),
+    )(residual, part, gain)
+
+
+def scatter_kernel(
+    line, terms, mixed, out, held, from_side, from_near, from_line,
+    cs, cr, bs, br, as_, ar, zs, zr, fs, fr,
+):
+    s, c, z, p, near, side, far = places()
+    to_near = (z * PLANE + near, c)
+    to_side = (z * PLANE + side, c)
+    to_core = (s, 1 - c)
+    meet(
+        [to_near, to_side, to_core]
+        + [(((z + j) % line) * PLANE + p, c) for j in range(1, line)]
+    )
+    sends = []
+
+    def send(*args):
+        copy = remote(*args)
+        copy.start()
+        sends.append(copy)
+
+    def arrived(block, send_sem, recv_sem):
+        remote(block, block, send_sem, recv_sem, to_core).wait_recv()
+
+    def add(a, b):
+        return (a.astype(jnp.float32) + b.astype(jnp.float32)).astype(jnp.bfloat16)
+
+    order = list(range(1, line)) + [0]
+    for j in order:
+        send(terms.at[(z + j) % line, :, 1 - c], held.at[j], cs.at[j], cr.at[j], to_core)
+
+    def stage_core(j):
+        arrived(held.at[j], cs.at[j], cr.at[j])
+        zt = (z + j) % line
+        for place in (side, far):
+            held[j, place] = add(held[j, place], terms[zt, place, c])
+        send(held.at[j, side], from_side.at[j, 0], bs.at[j, 0], br.at[j, 0], to_side)
+        send(held.at[j, far], from_side.at[j, 1], bs.at[j, 1], br.at[j, 1], to_side)
+        for place in (p, near):
+            held[j, place] = add(held[j, place], terms[zt, place, c])
+
+    def stage_side(j):
+        arrived(from_side.at[j, 1], bs.at[j, 1], br.at[j, 1])
+        held[j, near] = add(held[j, near], from_side[j, 1])
+        send(held.at[j, near], from_near.at[j], as_.at[j], ar.at[j], to_near)
+        arrived(from_side.at[j, 0], bs.at[j, 0], br.at[j, 0])
+        held[j, p] = add(held[j, p], from_side[j, 0])
+
+    def stage_near(j):
+        arrived(from_near.at[j], as_.at[j], ar.at[j])
+        held[j, p] = add(held[j, p], from_near[j])
+        if j:
+            send(
+                held.at[j, p], from_line.at[j - 1], zs.at[j], zr.at[j],
+                (((z + j) % line) * PLANE + p, c),
+            )
+
+    for step in range(line + 2):
+        if step < line:
+            stage_core(order[step])
+        if 1 <= step <= line:
+            stage_side(order[step - 1])
+        if step >= 2:
+            stage_near(order[step - 2])
+    total = held[0, p].astype(jnp.float32)
+    for j in range(1, line):
+        arrived(from_line.at[j - 1], zs.at[j], zr.at[j])
+        total = total + from_line[j - 1].astype(jnp.float32)
+    out[c] = (mixed[...].astype(jnp.float32) + total).astype(jnp.bfloat16)
+    send(out.at[c], out.at[c], fs, fr, to_core)
+    arrived(out.at[1 - c], fs, fr)
+    for copy in sends:
+        copy.wait_send()
+
+
+def scatter_sum(line, terms, mixed):
+    dma = pltpu.SemaphoreType.DMA
+    vmem = pl.BlockSpec(memory_space=pltpu.VMEM)
+    half, features = mixed.shape
+    block = (half, features)
+    return pl.pallas_call(
+        functools.partial(scatter_kernel, line),
+        out_shape=jax.ShapeDtypeStruct((2,) + block, jnp.bfloat16),
+        in_specs=[vmem] * 2,
+        out_specs=vmem,
+        scratch_shapes=[
+            pltpu.VMEM((line, PLANE) + block, jnp.bfloat16),
+            pltpu.VMEM((line, 2) + block, jnp.bfloat16),
+            pltpu.VMEM((line,) + block, jnp.bfloat16),
+            pltpu.VMEM((line - 1,) + block, jnp.bfloat16),
+            dma((line,)), dma((line,)), dma((line, 2)), dma((line, 2)),
+            dma((line,)), dma((line,)), dma((line,)), dma((line,)), dma, dma,
+        ],
+        compiler_params=pltpu.CompilerParams(
+            collective_id=3, has_side_effects=True, vmem_limit_bytes=40 * 1024 * 1024
+        ),
+    )(terms, mixed)
+
+
+def placed_body(
+    residual, query_first, key_first, value_first, query_second, key_second, value_second,
+    balance_first, balance_second, head_gain_first, head_gain_second, out_first, out_second,
+    mlp_gain, up_weight, down_weight,
+):
+    tokens, line, wide = query_first.shape
+    features = residual.shape[1]
+    deep = value_second.shape[2]
+    half = tokens // 2
+    z = lax.axis_index("sp") // PLANE
+    empty = jnp.zeros((tokens, line, wide - query_second.shape[2]), jnp.bfloat16)
+    q = jnp.concatenate([query_first, query_second, empty], axis=-1).transpose(1, 0, 2)
+    kv = jnp.concatenate([key_first, value_first, key_second, value_second], axis=-1)
+    kv = kv.transpose(1, 0, 2)
+    kv_all, q_all, up_all, down_all = exchange(line, kv, q, up_weight, down_weight)
+    balance = jnp.stack([balance_first[z], balance_second[z]])
+    heads = attention(
+        line, wide // 2, query_second.shape[2] // 2, balance, q_all,
+        kv_all.reshape(-1, kv.shape[2]), head_gain_first[None, :], head_gain_second[None, :],
+    )
+    heads = return_heads(line, heads)
+    heads_first = heads[:, :, :wide].transpose(1, 0, 2).reshape(tokens, line * wide)
+    heads_second = heads[:, :, wide:].transpose(1, 0, 2).reshape(tokens, line * deep)
+    part = jnp.dot(heads_first, out_first, preferred_element_type=jnp.float32) + jnp.dot(
+        heads_second, out_second, preferred_element_type=jnp.float32
+    )
+    part = part.astype(jnp.bfloat16).reshape(2, half, features)
+    mixed, rows = gather_rows(line, residual.reshape(2, half, features), part, mlp_gain[None, :])
+    up = up_all.reshape(-1, up_all.shape[2])
+    down = down_all.reshape(-1, down_all.shape[2])
+    lifted = jnp.dot(rows.reshape(-1, features), up, preferred_element_type=jnp.float32)
+    active = jax.nn.relu(lifted)
+    hidden = (active * active).astype(jnp.bfloat16)
+    terms = last(hidden, down).astype(jnp.bfloat16)
+    out = scatter_sum(line, terms.reshape(line, PLANE, 2, half, features), mixed)
+    return out.reshape(tokens, features)
+
+
+def placed(mesh):
+    ranks = mesh.shape["sp"]
+    cores = mesh.shape["tp"]
+    return cores == 2 and ranks % PLANE == 0
+
+
+def choose(mesh):
+    ranks = mesh.shape["sp"]
+
+    def run(*arrays):
+        query_first, query_second, value_second, value_first = arrays[1], arrays[4], arrays[6], arrays[3]
+        fits = (
+            placed(mesh)
+            and query_first.shape[1] * PLANE == ranks
+            and query_second.shape[1] == query_first.shape[1]
+            and value_first.shape[2] == query_first.shape[2] == 128
+            and query_second.shape[2] + value_second.shape[2] == query_first.shape[2]
+            and query_first.shape[0] % 32 == 0
+            and arrays[14].shape[1] % (128 * ranks) == 0
+        )
+        return (placed_body if fits else body)(*arrays)
+
+    return run
+
+
 def solution(mesh):
     in_specs = (
         P("sp", None),
@@ -138,4 +603,4 @@
         P("sp", "tp"),
     )
     out_specs = P("sp", None)
-    return jax.shard_map(body, mesh=mesh, in_specs=in_specs, out_specs=out_specs, check_vma=False)
+    return jax.shard_map(choose(mesh), mesh=mesh, in_specs=in_specs, out_specs=out_specs, check_vma=False)

time: 705 us -> 234 us (0.33)
  waiting for transfers between devices: 650 us -> 0 us
  Pallas kernels: 0 us -> 189 us
  local copies, waits for them, and re-layouts: 7.12 us -> 25.5 us
  between operations: 13.7 us -> 0.15 us
  matrix products: 27.9 us -> 15.5 us
    all_gather x6 -> x0, waiting for transfers between devices: 604 us -> none  [the longest x1 194 us: body(): lax.all_gather(up_weight, 'sp', axis=0, tiled=True)]
    pallas_call x0 -> x5, Pallas kernels: none -> 189 us  [the longest x1 55.9 us: scatter_sum(): pl.pallas_call(functools.partial(scatter_kernel, line), out_shape=jax.Sha...]
    psum x2 -> x0, waiting for transfers between devices: 42.7 us -> none  [the longest x1 25.8 us: body(): lax.psum(head_term.astype(jnp.bfloat16), 'tp').astype(jnp.float32)]
    unnamed x18 -> x31, local copies, waits for them, and re-layouts: 2.74 us -> 20.7 us
    dot_general x9 -> x3, matrix products: 27.9 us -> 15.5 us  [the longest x1 13.4 us: last(): lax.dot_general(a, b, (((1,), (1,)), ((), ())), preferred_element_type=jn...]
  transfers between devices with their start and end apart: 8 -> 0, of which waited for: 8 -> 0; matrix products, arithmetic and copies ran while one was open for 2% -> 0% of each run, Pallas kernels for 0% -> 0%
where the time goes in v1:
time: 234 us
  Pallas kernels  189 us (81%)
  local copies, waits for them, and re-layouts  25.5 us (11%)
  matrix products  15.5 us (7%)
  other arithmetic  3.45 us (1%)
    pallas_call x1, Pallas kernels, scatter_sum(): pl.pallas_call(functools.partial(scatter_kernel, line), out_shape=jax.Sha...  55.9 us
    pallas_call x1, Pallas kernels, exchange(): pl.pallas_call(functools.partial(exchange_kernel, line), out_shape=(jax.S...  52.4 us
    pallas_call x1, Pallas kernels, gather_rows(): pl.pallas_call(functools.partial(gather_kernel, line), out_shape=(jax.Sha...  47.6 us
    pallas_call x1, Pallas kernels, return_heads(): pl.pallas_call(functools.partial(return_kernel, line), out_shape=jax.Shap...  26.3 us
    unnamed x31, local copies, waits for them, and re-layouts  20.7 us
    dot_general x1, matrix products, last(): lax.dot_general(a, b, (((1,), (1,)), ((), ())), preferred_element_type=jn...  13.4 us
    pallas_call x1, Pallas kernels, attention(): pl.pallas_call(functools.partial(attention_kernel, line, size_a, size_b),...  6.77 us

profile of v1, /device:TPU:0, one launch (start us, length us, event | category | flops | bytes accessed | tf_op | source)
XLA Modules:
  0.0 233.6 jit_solution(7779241872035436652)
XLA Ops:
  0.0 1.4 dynamic_slice.7
  1.4 1.2 dynamic_slice.6
  2.6 1.3 pad_maximum_fusion.balance
  3.9 0.1 pad.2.clone
  4.0 1.6 copy.27
  5.6 0.9 copy.23
  6.5 1.6 copy.24
  8.1 1.6 copy.28
  9.7 1.0 maximum_bitcast_fusion.1.q
  10.7 1.6 copy.25
  12.3 1.6 copy.26
  13.9 1.1 maximum_bitcast_fusion.kv
  15.1 1.2 copy-done.4
  16.3 52.4 %shard_map.154 = (bf16[16,128,384]{2,1,0:T(8,128)(2,1)S(1)}, bf16[4,128,256]{2,1,0:T(8,128)(2,1)S(1)}, bf16[16,128,256]{2,1,0:T(8,128)(2,1)S(1)}, bf16[16,128,256]{2,1,0:T(8,128)(2,1)S(1)}) custom-call(bf16[4,128,384]{2,1,0:T(8,128)(2,1)S(1)} %maximum_bitcast_fusion.kv, bf16[4,128,256]{2,1,0:T(8,128)(2,1)S(1)} %maximum_bitcast_fusion.1.q, ...), custom_call_target="tpu_custom_call" | custom-call | tf_op jit(solution)/shard_map/pallas_call | solution.py:237
  68.7 1.0 copy-done.10
  69.7 1.0 copy-done.11
  70.7 6.8 %shard_map.155.heads = bf16[4,128,192]{2,1,0:T(8,128)(2,1)S(1)} custom-call(f32[2]{0:T(128)S(1)} %pad_maximum_fusion.balance, bf16[4,128,256]{2,1,0:T(8,128)(2,1)S(1)} %get-tuple-element.11.q, bf16[2048,384]{1,0:T(8,128)(2,1)S(1)} %bitcast.31, f32[1,128]{1,0:T(1,128)S(1)} %bitcast.34, f32[1,64]{1,0:T(1,128)S(1)} %bitcast.35), custom_call_target="tpu_custom_call" | custom-call | tf_op jit(solution)/shard_map/pallas_call | solution.py:304
  77.5 0.7 copy-done.2
  78.2 26.3 %shard_map.156 = bf16[4,128,192]{2,1,0:T(8,128)(2,1)} custom-call(bf16[4,128,192]{2,1,0:T(8,128)(2,1)} %copy-done.2), custom_call_target="tpu_custom_call" | custom-call | tf_op jit(solution)/shard_map/pallas_call | solution.py:335
  104.5 0.9 slice_bitcast_fusion
  105.4 0.9 slice_bitcast_fusion.1
  106.3 0.1 copy.30
  106.4 0.1 copy.29
  106.5 1.6 fusion.5
  108.1 0.5 fusion.2
  108.6 0.5 copy-done.5
  109.2 47.6 %shard_map.157 = (bf16[64,2048]{1,0:T(8,128)(2,1)S(1)}, bf16[32,64,2048]{2,1,0:T(8,128)(2,1)S(1)}) custom-call(bf16[2,64,2048]{2,1,0:T(8,128)(2,1)S(1)} %bitcast.32, bf16[2,64,2048]{2,1,0:T(8,128)(2,1)S(1)} %bitcast.30, f32[1,2048]{1,0:T(1,128)S(1)} %bitcast.33), custom_call_target="tpu_custom_call" | custom-call | tf_op jit(solution)/shard_map/pallas_call | solution.py:408
  156.8 3.2 %copy-done.9 = bf16[32,64,2048]{2,1,0:T(8,128)(2,1)} copy-done((bf16[32,64,2048]{2,1,0:T(8,128)(2,1)}, bf16[32,64,2048]{2,1,0:T(8,128)(2,1)S(1)}, u32[]{:S(2)}) %copy-start.9) | copy-done | bytes 8388632
  160.0 13.4 %convolution_convert_fusion = bf16[2048,2048]{1,0:T(8,128)(2,1)} fusion(bf16[2048,256]{1,0:T(8,128)(2,1)} %bitcast.38, bf16[2048,2048]{1,0:T(8,128)(2,1)} %bitcast.36, bf16[2048,256]{1,0:T(8,128)(2,1)} %bitcast.37), kind=kOutput, calls=%fused_computation | convolution fusion | flops 4300734464 | bytes 18874368 | tf_op jit(solution)/shard_map/dot_general | solution.py:258
  173.4 3.4 %copy-done.1 = bf16[2048,2048]{1,0:T(8,128)(2,1)S(1)} copy-done((bf16[2048,2048]{1,0:T(8,128)(2,1)S(1)}, bf16[2048,2048]{1,0:T(8,128)(2,1)}, u32[]{:S(2)}) %copy-start.1) | copy-done | bytes 8388632
  176.8 55.9 %shard_map.158 = bf16[2,64,2048]{2,1,0:T(8,128)(2,1)S(1)} custom-call(bf16[4,4,2,64,2048]{4,3,2,1,0:T(8,128)(2,1)S(1)} %bitcast.28, bf16[64,2048]{1,0:T(8,128)(2,1)S(1)} %get-tuple-element.16.mixed), custom_call_target="tpu_custom_call" | custom-call | tf_op jit(solution)/shard_map/pallas_call | solution.py:504
  232.8 0.8 copy.32
  (18 shorter events, 0.0 us)
Async XLA Ops:
  0.0 108.1 %copy-start = (bf16[512,2048]{1,0:T(8,128)(2,1)S(1)}, bf16[512,2048]{1,0:T(8,128)(2,1)}, u32[]{:S(2)}) copy-start(bf16[512,2048]{1,0:T(8,128)(2,1)} %param.27) | copy-start | bytes 6291460
  0.0 15.1 %copy-start.3 = (bf16[128,4096]{1,0:T(8,128)(2,1)S(1)}, bf16[128,4096]{1,0:T(8,128)(2,1)}, u32[]{:S(2)}) copy-start(bf16[128,4096]{1,0:T(8,128)(2,1)} %up.1) | copy-start | bytes 3145732
  10.7 60.0 %copy-start.7 = (f32[128]{0:T(128)S(1)}, f32[128]{0:T(128)}, u32[]{:S(2)}) copy-start(f32[128]{0:T(128)} %param.25) | copy-start | bytes 1540
  10.7 60.0 %copy-start.8 = (f32[64]{0:T(128)S(1)}, f32[64]{0:T(128)}, u32[]{:S(2)}) copy-start(f32[64]{0:T(128)} %param.26) | copy-start | bytes 772
  15.1 1.2 copy-start.4
  68.7 1.0 copy-start.10
  69.7 1.0 copy-start.11
  77.5 0.7 copy-start.2
  108.1 1.0 copy-start.5
  108.1 1.0 copy-start.6
  156.8 3.2 %copy-start.9 = (bf16[32,64,2048]{2,1,0:T(8,128)(2,1)}, bf16[32,64,2048]{2,1,0:T(8,128)(2,1)S(1)}, u32[]{:S(2)}) copy-start(bf16[32,64,2048]{2,1,0:T(8,128)(2,1)S(1)} %get-tuple-element.13) | copy-start | bytes 25165828
  173.4 3.4 %copy-start.1 = (bf16[2048,2048]{1,0:T(8,128)(2,1)S(1)}, bf16[2048,2048]{1,0:T(8,128)(2,1)}, u32[]{:S(2)}) copy-start(bf16[2048,2048]{1,0:T(8,128)(2,1)} %convolution_convert_fusion) | copy-start | bytes 25165828

commit v2 on v0

--- a/solution.py
+++ b/solution.py
@@ -1,8 +1,11 @@
+import functools
 import math
 
 import jax
 import jax.numpy as jnp
 from jax import lax
+from jax.experimental import pallas as pl
+from jax.experimental.pallas import tpu as pltpu
 from jax.sharding import PartitionSpec as P
 
 DK_A = 64
@@ -118,6 +121,405 @@
     return (mixed_float + added).astype(jnp.bfloat16)
 
 
+PLANE = 4
+MESH = pl.DeviceIdType.MESH
+VMEM_BYTES = 60 * 1024 * 1024
+
+
+def remote(src, dst, send_sem, recv_sem, device):
+    return pltpu.make_async_remote_copy(
+        src_ref=src, dst_ref=dst, send_sem=send_sem, recv_sem=recv_sem,
+        device_id=device, device_id_type=MESH,
+    )
+
+
+def meet(devices):
+    barrier = pltpu.get_barrier_semaphore()
+    for device in devices:
+        pl.semaphore_signal(barrier, inc=1, device_id=device, device_id_type=MESH)
+    pl.semaphore_wait(barrier, len(devices))
+
+
+def places():
+    s = lax.axis_index("sp")
+    c = lax.axis_index("tp")
+    z = s // PLANE
+    p = s % PLANE
+    x = p % 2
+    y = p // 2
+    flip_x = y * 2 + 1 - x
+    flip_y = (1 - y) * 2 + x
+    near = (1 - c) * flip_x + c * flip_y
+    side = (1 - c) * flip_y + c * flip_x
+    far = (1 - y) * 2 + 1 - x
+    return s, c, z, p, near, side, far
+
+
+def last(a, b):
+    return lax.dot_general(a, b, (((1,), (1,)), ((), ())), preferred_element_type=jnp.float32)
+
+
+def add(a, b):
+    return (a.astype(jnp.float32) + b.astype(jnp.float32)).astype(jnp.bfloat16)
+
+
+def attend_line(line, p, size_a, size_b, balance_a, balance_b, q, kv, gain_a, gain_b, out):
+    tokens = q.shape[1]
+    wide = gain_a.shape[1]
+    deep = gain_b.shape[1]
+    span = PLANE * tokens
+    lanes = lax.broadcasted_iota(jnp.int32, (tokens, wide), 1)
+    rows = lax.broadcasted_iota(jnp.int32, (tokens, span), 0) + p * tokens
+    visible = lax.broadcasted_iota(jnp.int32, (tokens, span), 1) <= rows
+
+    def mix(queries, keys_at, values_at, size, b, keys_number):
+        maps = []
+        for m in range(2):
+            chosen = (lanes >= m * size) & (lanes < (m + 1) * size)
+            picked = jnp.where(chosen, queries, jnp.zeros_like(queries))
+            scores = last(picked, kv[0:keys_number, keys_at]) * size ** (-0.5)
+            tail_scores = jnp.where(visible, scores[:, keys_number - span:], -jnp.inf)
+            if keys_number > span:
+                scores = jnp.concatenate([scores[:, : keys_number - span], tail_scores], axis=1)
+            else:
+                scores = tail_scores
+            powers = jnp.exp(scores - jnp.max(scores, axis=-1, keepdims=True))
+            maps.append((powers, jnp.sum(powers, axis=-1, keepdims=True)))
+        (e1, l1), (e2, l2) = maps
+        weights = (e1 * (1.0 / l1) - e2 * (b / l2)).astype(jnp.bfloat16)
+        return jnp.dot(weights, kv[0:keys_number, values_at], preferred_element_type=jnp.float32)
+
+    def norm(mixed, gain):
+        power = jnp.mean(mixed * mixed, axis=-1, keepdims=True)
+        return (mixed * lax.rsqrt(power + EPSILON) * gain[...] * HEAD_SCALE).astype(jnp.bfloat16)
+
+    for j in range(line):
+        number = (j + 1) * span
+        first = mix(q[j, :, 0:wide], slice(0, wide), slice(wide, 2 * wide), size_a, balance_a, number)
+        out[j, :, 0:wide] = norm(first, gain_a)
+        both = slice(2 * wide, 3 * wide)
+        second = mix(q[j, :, wide:2 * wide], both, both, size_b, balance_b, number)
+        out[j, :, wide:wide + deep] = norm(second[:, wide - deep:wide], gain_b)
+
+
+def layer_kernel(
+    line, size_a, size_b, balance_a, balance_b, kv, q, gain_a, gain_b, gain, residual,
+    out_a, out_b, up, down, out,
+    kv_all, q_all, up_all, down_all, heads, gathered, part, other_part, mixed,
+    rows, terms, held, from_side, from_near, from_line, projections_a, projections_b,
+    local, kzs, kzr, qs, qr, kps, kpr, us, ur, ds, dr, hs, hr, xs, xr,
+    gzs, gzr, gps, gpr, gcs, gcr, tcs, tcr, tbs, tbr, tas, tar, tzs, tzr, fs, fr,
+):
+    s, c, z, p, near, side, far = places()
+    n = line * PLANE
+    tokens = kv.shape[1]
+    width = up_all.shape[1]
+    depth = up.shape[0]
+    half = tokens // 2
+    features = residual.shape[2]
+    wide = gain_a.shape[1]
+    deep = gain_b.shape[1]
+    to_near = (z * PLANE + near, c)
+    to_side = (z * PLANE + side, c)
+    to_core = (s, 1 - c)
+    meet([((s + k) % n, c) for k in range(1, n)] + [to_core])
+    sends = []
+
+    def send(*args):
+        copy = remote(*args)
+        copy.start()
+        sends.append(copy)
+
+    def arrived(block, send_sem, recv_sem):
+        remote(block, block, send_sem, recv_sem, to_core).wait_recv()
+
+    def in_line(j):
+        return (((z + j) % line) * PLANE + p, c)
+
+    def before(j):
+        return (z + line - j) % line
+
+    def tokens_of(place):
+        return kv_all.at[pl.ds(pl.multiple_of(place * tokens, tokens), tokens)]
+
+    def share_of(ref, place):
+        return ref.at[pl.ds(pl.multiple_of(place * depth, depth), depth)]
+
+    def columns_of(place):
+        return pl.ds(pl.multiple_of(place * width, width), width)
+
+    for j in range(1, line):
+        zt = (z + j) % line
+        send(kv.at[zt], tokens_of(s), kzs.at[j], kzr.at[j], in_line(j))
+    locals_ = [
+        pltpu.make_async_copy(kv.at[z], tokens_of(s), local.at[0]),
+        pltpu.make_async_copy(q.at[z], q_all.at[z], local.at[1]),
+        pltpu.make_async_copy(up.at[:, columns_of(s)], share_of(up_all, s), local.at[2]),
+        pltpu.make_async_copy(down.at[:, columns_of(s)], share_of(down_all, s), local.at[3]),
+        pltpu.make_async_copy(out_a, projections_a, local.at[4]),
+        pltpu.make_async_copy(out_b, projections_b, local.at[5]),
+    ]
+    for copy in locals_:
+        copy.start()
+    locals_[0].wait()
+    for j in range(line):
+        block = tokens_of(before(j) * PLANE + p)
+        if j:
+            arrived(block, kzs.at[j], kzr.at[j])
+        send(block, block, kps.at[j, 0], kpr.at[j, 0], to_near)
+        send(block, block, kps.at[j, 1], kpr.at[j, 1], to_side)
+        if j == 0:
+            for i in range(1, line):
+                send(q.at[(z + i) % line], q_all.at[z], qs.at[i], qr.at[i], in_line(i))
+            for i in range(1, line):
+                k = i * PLANE
+                send(
+                    up.at[:, columns_of((s + k) % n)], share_of(up_all, s),
+                    us.at[k], ur.at[k], ((s + k) % n, c),
+                )
+    for j in range(line):
+        block = tokens_of(before(j) * PLANE + near)
+        arrived(block, kps.at[j, 0], kpr.at[j, 0])
+        send(block, block, kps.at[j, 2], kpr.at[j, 2], to_side)
+    for k in range(1, n):
+        if k % PLANE:
+            send(
+                up.at[:, columns_of((s + k) % n)], share_of(up_all, s),
+                us.at[k], ur.at[k], ((s + k) % n, c),
+            )
+    for j in range(line):
+        for way, place in ((1, side), (2, far)):
+            arrived(tokens_of(before(j) * PLANE + place), kps.at[j, way], kpr.at[j, way])
+    for j in range(1, line):
+        arrived(q_all.at[before(j)], qs.at[j], qr.at[j])
+    locals_[1].wait()
+
+    attend_line(
+        line, p, size_a, size_b, balance_a[z], balance_b[z], q_all, kv_all, gain_a, gain_b, heads
+    )
+
+    for j in range(1, line):
+        send(heads.at[(z + j) % line], gathered.at[z], hs.at[j], hr.at[j], in_line(j))
+    mine = pltpu.make_async_copy(heads.at[z], gathered.at[z], local.at[6])
+    mine.start()
+    mine.wait()
+    for copy in locals_[2:]:
+        copy.wait()
+    for j in range(1, line):
+        arrived(gathered.at[before(j)], hs.at[j], hr.at[j])
+    firsts = jnp.concatenate([gathered[h, :, 0:wide] for h in range(line)], axis=1)
+    seconds = jnp.concatenate([gathered[h, :, wide:wide + deep] for h in range(line)], axis=1)
+    step = features // 4
+    for i in range(4):
+        columns = slice(i * step, (i + 1) * step)
+        value = jnp.dot(firsts, projections_a[:, columns], preferred_element_type=jnp.float32)
+        value = value + jnp.dot(seconds, projections_b[:, columns], preferred_element_type=jnp.float32)
+        value = value.astype(jnp.bfloat16)
+        part[0, :, columns] = value[:half]
+        part[1, :, columns] = value[half:]
+    swap = remote(part.at[1 - c], other_part, xs, xr, to_core)
+    swap.start()
+    swap.wait()
+    total = part[c].astype(jnp.float32) + other_part[...].astype(jnp.float32)
+    mixed[...] = (residual[c].astype(jnp.float32) + total).astype(jnp.bfloat16)
+    whole = mixed[...].astype(jnp.float32)
+    power = jnp.mean(whole * whole, axis=-1, keepdims=True)
+    rows[s * 2 + c] = (whole * lax.rsqrt(power + EPSILON) * gain[...]).astype(jnp.bfloat16)
+
+    def slot(j, place, core):
+        return rows.at[(before(j) * PLANE + place) * 2 + core]
+
+    def pass_on(block, send_sem, recv_sem, device):
+        send(block, block, send_sem, recv_sem, device)
+
+    for j in range(1, line):
+        pass_on(slot(0, p, c), gzs.at[j], gzr.at[j], in_line(j))
+    for j in range(line + 1):
+        if j < line:
+            block = slot(j, p, c)
+            if j:
+                arrived(block, gzs.at[j], gzr.at[j])
+            pass_on(block, gps.at[j, 0], gpr.at[j, 0], to_near)
+            pass_on(block, gps.at[j, 1], gpr.at[j, 1], to_side)
+            pass_on(block, gcs.at[j, 0], gcr.at[j, 0], to_core)
+            if j == 0:
+                for k in range(1, n):
+                    send(
+                        down.at[:, columns_of((s + k) % n)], share_of(down_all, s),
+                        ds.at[k], dr.at[k], ((s + k) % n, c),
+                    )
+        if j:
+            block = slot(j - 1, near, c)
+            arrived(block, gps.at[j - 1, 0], gpr.at[j - 1, 0])
+            pass_on(block, gps.at[j - 1, 2], gpr.at[j - 1, 2], to_side)
+            pass_on(block, gcs.at[j - 1, 1], gcr.at[j - 1, 1], to_core)
+
+    def rows_here(j):
+        for way, place in ((1, side), (2, far)):
+            block = slot(j, place, c)
+            arrived(block, gps.at[j, way], gpr.at[j, way])
+            pass_on(block, gcs.at[j, 1 + way], gcr.at[j, 1 + way], to_core)
+
+    def mixer(j):
+        for way, place in enumerate((p, side, near, far)):
+            arrived(slot(j, place, 1 - c), gcs.at[j, way], gcr.at[j, way])
+        if j == 0:
+            for k in range(1, n):
+                f = (s + n - k) % n
+                arrived(share_of(up_all, f), us.at[k], ur.at[k])
+                arrived(share_of(down_all, f), ds.at[k], dr.at[k])
+        first = before(j) * PLANE * 2
+        block = rows[pl.ds(first, PLANE * 2)].reshape(PLANE * 2 * half, features)
+        active = jnp.maximum(jnp.dot(block, up_all[...], preferred_element_type=jnp.float32), 0.0)
+        hidden = (active * active).astype(jnp.bfloat16)
+        for i in range(4):
+            value = last(hidden, down_all[i * step:(i + 1) * step, :]).astype(jnp.bfloat16)
+            terms[j, :, :, :, i * step:(i + 1) * step] = value.reshape(PLANE, 2, half, step)
+        send(terms.at[j, :, 1 - c], held.at[j], tcs.at[j], tcr.at[j], to_core)
+
+    def stage_core(j):
+        arrived(held.at[j], tcs.at[j], tcr.at[j])
+        for place in (side, far):
+            held[j, place] = add(held[j, place], terms[j, place, c])
+        send(held.at[j, side], from_side.at[j, 0], tbs.at[j, 0], tbr.at[j, 0], to_side)
+        send(held.at[j, far], from_side.at[j, 1], tbs.at[j, 1], tbr.at[j, 1], to_side)
+        for place in (p, near):
+            held[j, place] = add(held[j, place], terms[j, place, c])
+
+    def stage_side(j):
+        arrived(from_side.at[j, 1], tbs.at[j, 1], tbr.at[j, 1])
+        held[j, near] = add(held[j, near], from_side[j, 1])
+        send(held.at[j, near], from_near.at[j], tas.at[j], tar.at[j], to_near)
+        arrived(from_side.at[j, 0], tbs.at[j, 0], tbr.at[j, 0])
+        held[j, p] = add(held[j, p], from_side[j, 0])
+
+    def stage_near(j):
+        arrived(from_near.at[j], tas.at[j], tar.at[j])
+        held[j, p] = add(held[j, p], from_near[j])
+        if j:
+            send(
+                held.at[j, p], from_line.at[j - 1], tzs.at[j], tzr.at[j],
+                (before(j) * PLANE + p, c),
+            )
+
+    for turn in range(line + 4):
+        if turn < line:
+            rows_here(turn)
+        if 1 <= turn <= line:
+            mixer(turn - 1)
+        if 2 <= turn <= line + 1:
+            stage_core(turn - 2)
+        if 3 <= turn <= line + 2:
+            stage_side(turn - 3)
+        if turn >= 4:
+            stage_near(turn - 4)
+    summed = held[0, p].astype(jnp.float32)
+    for j in range(1, line):
+        arrived(from_line.at[j - 1], tzs.at[j], tzr.at[j])
+        summed = summed + from_line[j - 1].astype(jnp.float32)
+    out[c] = (mixed[...].astype(jnp.float32) + summed).astype(jnp.bfloat16)
+    send(out.at[c], out.at[c], fs, fr, to_core)
+    arrived(out.at[1 - c], fs, fr)
+    for copy in sends:
+        copy.wait_send()
+
+
+def layer(line, size_a, size_b, *arrays):
+    kv, q, residual, out_a, out_b, up = [arrays[i] for i in (2, 3, 7, 8, 9, 10)]
+    n = line * PLANE
+    width = up.shape[1] // n
+    _, half, features = residual.shape
+    block = (half, features)
+    dma = pltpu.SemaphoreType.DMA
+    vmem = pl.BlockSpec(memory_space=pltpu.VMEM)
+    smem = pl.BlockSpec(memory_space=pltpu.SMEM)
+    hbm = pl.BlockSpec(memory_space=pl.ANY)
+    wide = arrays[4].shape[1]
+    deep = arrays[5].shape[1]
+
+    def space(*shape):
+        return pltpu.VMEM(shape, jnp.bfloat16)
+
+    lines = dma((line,))
+    return pl.pallas_call(
+        functools.partial(layer_kernel, line, size_a, size_b),
+        out_shape=jax.ShapeDtypeStruct((2,) + block, jnp.bfloat16),
+        in_specs=[smem, smem] + [vmem] * 6 + [hbm] * 4,
+        out_specs=vmem,
+        scratch_shapes=[
+            space(n * kv.shape[1], kv.shape[2]),
+            space(*q.shape),
+            space(n * up.shape[0], width),
+            space(n * up.shape[0], width),
+            space(line, q.shape[1], wide + deep),
+            space(line, q.shape[1], wide + deep),
+            space(2, *block),
+            space(*block),
+            space(*block),
+            space(n * 2, *block),
+            space(line, PLANE, 2, *block),
+            space(line, PLANE, *block),
+            space(line, 2, *block),
+            space(line, *block),
+            space(line - 1, *block),
+            space(*out_a.shape),
+            space(*out_b.shape),
+            dma((7,)),
+            lines, lines, lines, lines, dma((line, 3)), dma((line, 3)),
+            dma((n,)), dma((n,)), dma((n,)), dma((n,)), lines, lines, dma, dma,
+            lines, lines, dma((line, 3)), dma((line, 3)), dma((line, 4)), dma((line, 4)),
+            lines, lines, dma((line, 2)), dma((line, 2)), lines, lines, lines, lines, dma, dma,
+        ],
+        compiler_params=pltpu.CompilerParams(
+            collective_id=0, has_side_effects=True, vmem_limit_bytes=VMEM_BYTES
+        ),
+    )(*arrays)
+
+
+def placed_body(
+    residual, query_first, key_first, value_first, query_second, key_second, value_second,
+    balance_first, balance_second, head_gain_first, head_gain_second, out_first, out_second,
+    mlp_gain, up_weight, down_weight,
+):
+    tokens, line, wide = query_first.shape
+    features = residual.shape[1]
+    empty = jnp.zeros((tokens, line, wide - query_second.shape[2]), jnp.bfloat16)
+    q = jnp.concatenate([query_first, query_second, empty], axis=-1).transpose(1, 0, 2)
+    kv = jnp.concatenate([key_first, value_first, key_second, value_second], axis=-1)
+    kv = kv.transpose(1, 0, 2)
+    out = layer(
+        line, wide // 2, query_second.shape[2] // 2, balance_first, balance_second, kv, q,
+        head_gain_first[None, :], head_gain_second[None, :], mlp_gain[None, :],
+        residual.reshape(2, tokens // 2, features), out_first, out_second, up_weight, down_weight,
+    )
+    return out.reshape(tokens, features)
+
+
+def placed(mesh):
+    ranks = mesh.shape["sp"]
+    cores = mesh.shape["tp"]
+    return cores == 2 and ranks % PLANE == 0
+
+
+def choose(mesh):
+    ranks = mesh.shape["sp"]
+
+    def run(*arrays):
+        query_first, query_second, value_second, value_first = arrays[1], arrays[4], arrays[6], arrays[3]
+        fits = (
+            placed(mesh)
+            and query_first.shape[1] * PLANE == ranks
+            and query_second.shape[1] == query_first.shape[1]
+            and value_first.shape[2] == query_first.shape[2] == 128
+            and query_second.shape[2] + value_second.shape[2] == query_first.shape[2]
+            and query_first.shape[0] % 32 == 0
+            and arrays[14].shape[1] % (128 * ranks) == 0
+        )
+        return (placed_body if fits else body)(*arrays)
+
+    return run
+
+
 def solution(mesh):
     in_specs = (
         P("sp", None),
@@ -138,4 +540,4 @@
         P("sp", "tp"),
     )
     out_specs = P("sp", None)
-    return jax.shard_map(body, mesh=mesh, in_specs=in_specs, out_specs=out_specs, check_vma=False)
+    return jax.shard_map(choose(mesh), mesh=mesh, in_specs=in_specs, out_specs=out_specs, check_vma=False)

time: 705 us -> 173 us (0.25)
  waiting for transfers between devices: 650 us -> 0 us
  Pallas kernels: 0 us -> 164 us
  matrix products: 27.9 us -> 0 us
  between operations: 13.7 us -> 0.04 us
    all_gather x6 -> x0, waiting for transfers between devices: 604 us -> none  [the longest x1 194 us: body(): lax.all_gather(up_weight, 'sp', axis=0, tiled=True)]
    pallas_call x0 -> x1, Pallas kernels: none -> 164 us  [layer(): pl.pallas_call(functools.partial(layer_kernel, line, size_a, size_b), out...]
    psum x2 -> x0, waiting for transfers between devices: 42.7 us -> none  [the longest x1 25.8 us: body(): lax.psum(head_term.astype(jnp.bfloat16), 'tp').astype(jnp.float32)]
    dot_general x9 -> x0, matrix products: 27.9 us -> none  [the longest x1 15.7 us: body(): lax.dot_general(hidden, down_whole, (((1,), (1,)), ((), ())), preferred_e...]
  transfers between devices with their start and end apart: 8 -> 0, of which waited for: 8 -> 0; matrix products, arithmetic and copies ran while one was open for 2% -> 0% of each run, Pallas kernels for 0% -> 0%
where the time goes in v2:
time: 173 us
  Pallas kernels  164 us (95%)
  local copies, waits for them, and re-layouts  7.62 us (4%)
    pallas_call x1, Pallas kernels, layer(): pl.pallas_call(functools.partial(layer_kernel, line, size_a, size_b), out...  164 us
    unnamed x7, local copies, waits for them, and re-layouts  7.53 us

profile of v2, /device:TPU:0, one launch (start us, length us, event | category | flops | bytes accessed | tf_op | source)
XLA Modules:
  0.0 172.9 jit_solution(2744538970749970494)
XLA Ops:
  0.0 0.1 pad.2.clone
  0.1 0.9 copy.21
  1.0 0.9 copy.17
  1.9 0.9 copy.18
  2.9 1.0 copy.22
  3.8 0.8 maximum_bitcast_fusion.1.q
  4.6 1.0 copy.19
  5.6 1.0 copy.20
  6.5 0.9 maximum_bitcast_fusion.kv
  7.4 163.7 %shard_map.154 = bf16[2,64,2048]{2,1,0:T(8,128)(2,1)} custom-call(f32[4]{0:T(128)} %balance_a.1, f32[4]{0:T(128)} %balance_b.1, bf16[4,128,384]{2,1,0:T(8,128)(2,1)} %maximum_bitcast_fusion.kv, bf16[4,128,256]{2,1,0:T(8,128)(2,1)} %maximum_bitcast_fusion.1.q, f32[1,128]{1,0:T(1,128)} %bitcast.12, f32[1,64]{1,0:T(1,128)} %bitcast.13, f32[1,2048]{1,0:T(1,128)} %bitcast.11, ...), custom_call_target="tpu_custom_call" | custom-call | tf_op jit(solution)/shard_map/pallas_call | solution.py:444
  171.1 1.9 %copy.24 = bf16[128,2048]{1,0:T(8,128)(2,1)} copy(bf16[128,2048]{1,0:T(8,128)(2,1)} %bitcast.9) | data formatting | bytes 1048576
  (1 shorter events, 0.0 us)

commit v3 on v2

--- a/solution.py
+++ b/solution.py
@@ -133,11 +133,11 @@
     )
 
 
-def meet(devices):
+def greet(devices):
     barrier = pltpu.get_barrier_semaphore()
     for device in devices:
         pl.semaphore_signal(barrier, inc=1, device_id=device, device_id_type=MESH)
-    pl.semaphore_wait(barrier, len(devices))
+    return functools.partial(pl.semaphore_wait, barrier, len(devices))
 
 
 def places():
@@ -203,9 +203,9 @@
 
 
 def layer_kernel(
-    line, size_a, size_b, balance_a, balance_b, kv, q, gain_a, gain_b, gain, residual,
-    out_a, out_b, up, down, out,
-    kv_all, q_all, up_all, down_all, heads, gathered, part, other_part, mixed,
+    line, size_a, size_b, balance_a, balance_b, query_a, key_a, value_a, query_b, key_b, value_b,
+    gain_a, gain_b, gain, residual, out_a, out_b, up, down, out,
+    kv, q, kv_all, q_all, up_all, down_all, heads, gathered, part, other_part, mixed,
     rows, terms, held, from_side, from_near, from_line, projections_a, projections_b,
     local, kzs, kzr, qs, qr, kps, kpr, us, ur, ds, dr, hs, hr, xs, xr,
     gzs, gzr, gps, gpr, gcs, gcr, tcs, tcr, tbs, tbr, tas, tar, tzs, tzr, fs, fr,
@@ -222,7 +222,12 @@
     to_near = (z * PLANE + near, c)
     to_side = (z * PLANE + side, c)
     to_core = (s, 1 - c)
-    meet([((s + k) % n, c) for k in range(1, n)] + [to_core])
+    met = greet([((s + k) % n, c) for k in range(1, n)] + [to_core])
+    for h in range(line):
+        kv[h, :, 0:wide] = key_a[:, h, :]
+        kv[h, :, wide:2 * wide] = value_a[:, h, :]
+        kv[h, :, 2 * wide:3 * wide] = jnp.concatenate([key_b[h], value_b[h]], axis=0).T
+    met()
     sends = []
 
     def send(*args):
@@ -259,6 +264,11 @@
         pltpu.make_async_copy(out_a, projections_a, local.at[4]),
         pltpu.make_async_copy(out_b, projections_b, local.at[5]),
     ]
+    for h in range(line):
+        q[h, :, 0:wide] = query_a[:, h, :]
+        queries = query_b[h]
+        empty = jnp.zeros((wide - queries.shape[0], tokens), queries.dtype)
+        q[h, :, wide:2 * wide] = jnp.concatenate([queries, empty], axis=0).T
     for copy in locals_:
         copy.start()
     locals_[0].wait()
@@ -300,6 +310,11 @@
 
     for j in range(1, line):
         send(heads.at[(z + j) % line], gathered.at[z], hs.at[j], hr.at[j], in_line(j))
+    for k in range(1, n):
+        send(
+            down.at[:, columns_of((s + k) % n)], share_of(down_all, s),
+            ds.at[k], dr.at[k], ((s + k) % n, c),
+        )
     mine = pltpu.make_async_copy(heads.at[z], gathered.at[z], local.at[6])
     mine.start()
     mine.wait()
@@ -342,12 +357,6 @@
             pass_on(block, gps.at[j, 0], gpr.at[j, 0], to_near)
             pass_on(block, gps.at[j, 1], gpr.at[j, 1], to_side)
             pass_on(block, gcs.at[j, 0], gcr.at[j, 0], to_core)
-            if j == 0:
-                for k in range(1, n):
-                    send(
-                        down.at[:, columns_of((s + k) % n)], share_of(down_all, s),
-                        ds.at[k], dr.at[k], ((s + k) % n, c),
-                    )
         if j:
             block = slot(j - 1, near, c)
             arrived(block, gps.at[j - 1, 0], gpr.at[j - 1, 0])
@@ -425,7 +434,8 @@
 
 
 def layer(line, size_a, size_b, *arrays):
-    kv, q, residual, out_a, out_b, up = [arrays[i] for i in (2, 3, 7, 8, 9, 10)]
+    query_a, residual, out_a, out_b, up = [arrays[i] for i in (2, 11, 12, 13, 14)]
+    tokens = query_a.shape[0]
     n = line * PLANE
     width = up.shape[1] // n
     _, half, features = residual.shape
@@ -434,8 +444,8 @@
     vmem = pl.BlockSpec(memory_space=pltpu.VMEM)
     smem = pl.BlockSpec(memory_space=pltpu.SMEM)
     hbm = pl.BlockSpec(memory_space=pl.ANY)
-    wide = arrays[4].shape[1]
-    deep = arrays[5].shape[1]
+    wide = arrays[8].shape[1]
+    deep = arrays[9].shape[1]
 
     def space(*shape):
         return pltpu.VMEM(shape, jnp.bfloat16)
@@ -444,15 +454,17 @@
     return pl.pallas_call(
         functools.partial(layer_kernel, line, size_a, size_b),
         out_shape=jax.ShapeDtypeStruct((2,) + block, jnp.bfloat16),
-        in_specs=[smem, smem] + [vmem] * 6 + [hbm] * 4,
+        in_specs=[smem, smem] + [vmem] * 10 + [hbm] * 4,
         out_specs=vmem,
         scratch_shapes=[
-            space(n * kv.shape[1], kv.shape[2]),
-            space(*q.shape),
+            space(line, tokens, 3 * wide),
+            space(line, tokens, 2 * wide),
+            space(n * tokens, 3 * wide),
+            space(line, tokens, 2 * wide),
             space(n * up.shape[0], width),
             space(n * up.shape[0], width),
-            space(line, q.shape[1], wide + deep),
-            space(line, q.shape[1], wide + deep),
+            space(line, tokens, wide + deep),
+            space(line, tokens, wide + deep),
             space(2, *block),
             space(*block),
             space(*block),
@@ -483,12 +495,10 @@
 ):
     tokens, line, wide = query_first.shape
     features = residual.shape[1]
-    empty = jnp.zeros((tokens, line, wide - query_second.shape[2]), jnp.bfloat16)
-    q = jnp.concatenate([query_first, query_second, empty], axis=-1).transpose(1, 0, 2)
-    kv = jnp.concatenate([key_first, value_first, key_second, value_second], axis=-1)
-    kv = kv.transpose(1, 0, 2)
+    second = [a.transpose(1, 2, 0) for a in (query_second, key_second, value_second)]
     out = layer(
-        line, wide // 2, query_second.shape[2] // 2, balance_first, balance_second, kv, q,
+        line, wide // 2, query_second.shape[2] // 2, balance_first, balance_second,
+        query_first, key_first, value_first, *second,
         head_gain_first[None, :], head_gain_second[None, :], mlp_gain[None, :],
         residual.reshape(2, tokens // 2, features), out_first, out_second, up_weight, down_weight,
     )

time: 173 us -> 178 us (1.029)
  Pallas kernels: 164 us -> 175 us
  local copies, waits for them, and re-layouts: 7.62 us -> 1.88 us
    pallas_call x1, Pallas kernels: 164 us -> 175 us  [layer(): pl.pallas_call(functools.partial(layer_kernel, line, size_a, size_b), out...]
    unnamed x7 -> x1, local copies, waits for them, and re-layouts: 7.53 us -> 1.88 us
where the time goes in v3:
time: 178 us; the launch traced here: 177 us
  Pallas kernels  175 us (98%)
  local copies, waits for them, and re-layouts  1.88 us (1%)
    pallas_call x1, Pallas kernels, layer(): pl.pallas_call(functools.partial(layer_kernel, line, size_a, size_b), out...  175 us

profile of v3, /device:TPU:0, one launch (start us, length us, event | category | flops | bytes accessed | tf_op | source)
XLA Modules:
  0.0 177.3 jit_solution(2951919829486252031)
XLA Ops:
  0.0 175.5 %shard_map.154 = bf16[2,64,2048]{2,1,0:T(8,128)(2,1)} custom-call(f32[4]{0:T(128)} %balance_a.1, f32[4]{0:T(128)} %balance_b.1, bf16[128,4,128]{2,1,0:T(4,128)(2,1)} %query_a.1, bf16[128,4,128]{2,1,0:T(4,128)(2,1)} %key_a.1, bf16[128,4,128]{2,1,0:T(4,128)(2,1)} %value_a.1, bf16[4,64,128]{2,1,0:T(8,128)(2,1)} %bitcast.10, bf16[4,64,128]{2,1,0:T(8,128)(2,1)} %bitcast.11, ...), custom_call_target="tpu_custom_call" | custom-call | tf_op jit(solution)/shard_map/pallas_call | solution.py:454
  175.5 1.9 %copy.18 = bf16[128,2048]{1,0:T(8,128)(2,1)} copy(bf16[128,2048]{1,0:T(8,128)(2,1)} %bitcast.8) | data formatting | bytes 1048576
